TPU v7x, 32 devices: a whole 2x2x4 slice. The times are simulated.
32 devices in a mesh: sp: 16 (over z, y, x), tp: 2 (over core).
Axes of the slice: x: 2, y: 2, z: 4, core: 2. Of those that a mesh axis runs over, the one named last changes fastest.
Arguments:
- residual: bfloat16 [2048, 2048], P(('sp', 'tp')), may hold values from -6 to 6
- query_wide: bfloat16 [2048, 1024], P('sp', 'tp'), may hold values from -6 to 6
- key_wide: bfloat16 [2048, 1024], P('sp', 'tp'), may hold values from -6 to 6
- value_wide: bfloat16 [2048, 2048], P('sp', 'tp'), may hold values from -6 to 6
- outgate_wide: bfloat16 [2048, 2048], P('sp', 'tp'), may hold values from -6 to 6
- gating_wide: float32 [3, 8, 2048], P(None, 'tp', 'sp'), may hold values from -4 to 240, as said below
- gain_wide: bfloat16 [2048], P('tp'), may hold values from 0.099609375 to 1.8984375
- readout_wide: bfloat16 [2048, 2048], P('tp'), may hold values from -0.109375 to 0.109375
- query_narrow: bfloat16 [2048, 512], P('sp', 'tp'), may hold values from -6 to 6
- key_narrow: bfloat16 [2048, 512], P('sp', 'tp'), may hold values from -6 to 6
- value_narrow: bfloat16 [2048, 1024], P('sp', 'tp'), may hold values from -6 to 6
- outgate_narrow: bfloat16 [2048, 1024], P('sp', 'tp'), may hold values from -6 to 6
- gating_narrow: float32 [3, 8, 2048], P(None, 'tp', 'sp'), may hold values from -4 to 240, as said below
- gain_narrow: bfloat16 [1024], P('tp'), may hold values from 0.099609375 to 1.8984375
- readout_narrow: bfloat16 [1024, 2048], P('tp'), may hold values from -0.109375 to 0.109375
- norm_gain: bfloat16 [2048], replicated, may hold values from 0.099609375 to 1.8984375
- gate_weight: bfloat16 [2048, 5632], P('sp', 'tp'), may hold values from -0.125 to 0.125
- up_weight: bfloat16 [2048, 5632], P('sp', 'tp'), may hold values from -0.125 to 0.125
- down_weight: bfloat16 [5632, 2048], P('tp', 'sp'), may hold values from -0.078125 to 0.078125
Outputs:
- mixed_out: bfloat16 [2048, 2048], P(('sp', 'tp'))
Inputs may be any that keep to these rules, and one draw needn't show every extreme that they name: `gating_wide`: row 0 holds input gate pre-activations, row 1 forget gate pre-activations, row 2 an added log-decay that is zero or negative. `gating_narrow`: row 0 holds input gate pre-activations, row 1 forget gate pre-activations, row 2 an added log-decay that is zero or negative.
All inputs are finite; a program needn't handle non-finite values.
Results may differ from a plain program's by a relative error of at most 0.017.
Values may be sent and summed in bfloat16 or wider, within the bound.
No kernel may reach another device: no remote copies, remote signals or barrier semaphores. Data moves between devices by JAX's collectives and lax.ppermute only.
A program may use at most 128 MiB of HBM per device.

v0:
```python
import jax
import jax.numpy as jnp
from jax import lax
from jax.sharding import PartitionSpec as P

DK_A = 128
DK_B = 64
BLOCK = 64


def entering(value, axis, combine, identity):
    length, here = (lax.axis_size(axis), lax.axis_index(axis))
    everything = jax.tree.map(lambda part: lax.all_gather(part, axis), value)
    start = jax.tree.map(
        lambda part, zero: jnp.broadcast_to(jnp.asarray(zero, part.dtype), part.shape),
        value,
        identity,
    )

    def step(k, before):
        reached = k < here
        new = combine(before, jax.tree.map(lambda part: part[k], everything))
        return jax.tree.map(lambda a, b: jnp.where(reached, a, b), new, before)

    return lax.fori_loop(0, length, step, start)


def local_pass(query, key_rows, value, gating, key_size):
    rows = query.shape[0]
    attention_tally = gating.shape[1]
    value_size = value.shape[1] // attention_tally
    nblocks = rows // BLOCK
    scale = key_size ** (-0.5)
    queries = query.reshape(nblocks, BLOCK, attention_tally, key_size)
    keys_all = key_rows.reshape(nblocks, BLOCK, attention_tally, key_size)
    values_all = value.reshape(nblocks, BLOCK, attention_tally, value_size)
    incoming_matrix = jnp.moveaxis(gating[0].reshape(attention_tally, nblocks, BLOCK), 1, 0)
    forget_log = jax.nn.log_sigmoid(gating[1]) + gating[2]
    forgets = jnp.moveaxis(forget_log.reshape(attention_tally, nblocks, BLOCK), 1, 0)
    causal = jnp.tril(jnp.ones((BLOCK, BLOCK), dtype=bool))

    def advance(carry, blocks):
        memory, level = carry
        q_block, k_block, v_block, in_block, f_block = blocks
        cumul = jnp.cumsum(f_block, axis=-1)
        logits = cumul[:, :, None] - cumul[:, None, :] + in_block[:, None, :]
        logits = jnp.where(causal, logits, -jnp.inf)
        carried = cumul + level[:, None]
        stab = jnp.maximum(carried, jnp.max(logits, axis=-1))
        weights = jnp.exp(logits - stab[:, :, None])
        scores = (
            jnp.einsum("thd,shd->hts", q_block, k_block, preferred_element_type=jnp.float32) * scale
        )
        weighted = (scores * weights).astype(jnp.bfloat16)
        within = jnp.einsum("hts,shv->thv", weighted, v_block, preferred_element_type=jnp.float32)
        earlier = jnp.einsum(
            "thd,hdv->thv", q_block.astype(jnp.float32), memory, precision=lax.Precision.HIGHEST
        )
        earlier = earlier * jnp.exp(carried - stab).T[:, :, None]
        last = cumul[:, -1]
        tail = last[:, None] - cumul + in_block
        level_new = jnp.maximum(last + level, jnp.max(tail, axis=-1))
        tail_weights = jnp.exp(tail - level_new[:, None]) * scale
        scaled_keys = (k_block * tail_weights.T[:, :, None]).astype(jnp.bfloat16)
        memory_new = jnp.exp(last + level - level_new)[:, None, None] * memory
        memory_new = memory_new + jnp.einsum(
            "shd,shv->hdv", scaled_keys, v_block, preferred_element_type=jnp.float32
        )
        return ((memory_new, level_new), (within + earlier, stab))

    init = (
        jnp.zeros((attention_tally, key_size, value_size), jnp.float32),
        jnp.full((attention_tally,), -1e30, jnp.float32),
    )
    (memory_end, level_end), (raw, stabs) = lax.scan(
        advance, init, (queries, keys_all, values_all, incoming_matrix, forgets)
    )
    raw = raw.reshape(rows, attention_tally, value_size)
    stabs = jnp.moveaxis(stabs, 0, 1).reshape(attention_tally, rows)
    running = jnp.cumsum(forget_log, axis=1)
    return (raw, stabs, running, memory_end, level_end, running[:, -1])


def merge_states(earlier, later):
    merged = []
    for group in range(2):
        memory_e, level_e, total_e = earlier[3 * group : 3 * group + 3]
        memory_l, level_l, total_l = later[3 * group : 3 * group + 3]
        level = jnp.maximum(level_e + total_l, level_l)
        memory = (
            jnp.exp(level_e + total_l - level)[:, None, None] * memory_e
            + jnp.exp(level_l - level)[:, None, None] * memory_l
        )
        merged.extend([memory, level, total_e + total_l])
    return tuple(merged)


def finish_group(query, raw, stabs, running, memory_in, level_in, gain, outgate, key_size):
    rows, attention_tally, value_size = raw.shape
    shifted = running + level_in[:, None]
    stab = jnp.maximum(stabs, shifted)
    own = raw * jnp.exp(stabs - stab).T[:, :, None]
    queries = query.reshape(rows, attention_tally, key_size).astype(jnp.float32)
    incoming = jnp.einsum("thd,hdv->thv", queries, memory_in, precision=lax.Precision.HIGHEST)
    total = own + incoming * jnp.exp(shifted - stab).T[:, :, None]
    normal_raw = total * lax.rsqrt(jnp.mean(total * total, axis=-1, keepdims=True) + 1e-06)
    flat = normal_raw.reshape(rows, attention_tally * value_size)
    flat = flat * gain.astype(jnp.float32) * jax.nn.sigmoid(outgate.astype(jnp.float32))
    return flat.astype(jnp.bfloat16)


def norm_rows(middle_f, norm_gain):
    normed = middle_f * lax.rsqrt(jnp.mean(middle_f * middle_f, axis=-1, keepdims=True) + 1e-06)
    return (normed * norm_gain.astype(jnp.float32)).astype(jnp.bfloat16)


def body(
    residual,
    query_wide,
    key_wide,
    value_wide,
    outgate_wide,
    gating_wide,
    gain_wide,
    readout_wide,
    query_narrow,
    key_narrow,
    value_narrow,
    outgate_narrow,
    gating_narrow,
    gain_narrow,
    readout_narrow,
    norm_gain,
    gate_weight,
    up_weight,
    down_weight,
):
    raw_w, stabs_w, running_w, memory_w, level_w, total_w = local_pass(
        query_wide, key_wide, value_wide, gating_wide, DK_A
    )
    raw_n, stabs_n, running_n, memory_n, level_n, total_n = local_pass(
        query_narrow, key_narrow, value_narrow, gating_narrow, DK_B
    )
    carried = entering(
        (memory_w, level_w, total_w, memory_n, level_n, total_n),
        "sp",
        merge_states,
        (
            jnp.zeros_like(memory_w),
            jnp.full_like(level_w, -1e30),
            jnp.zeros_like(total_w),
            jnp.zeros_like(memory_n),
            jnp.full_like(level_n, -1e30),
            jnp.zeros_like(total_n),
        ),
    )
    gated_w = finish_group(
        query_wide, raw_w, stabs_w, running_w, carried[0], carried[1], gain_wide, outgate_wide, DK_A
    )
    gated_n = finish_group(
        query_narrow,
        raw_n,
        stabs_n,
        running_n,
        carried[3],
        carried[4],
        gain_narrow,
        outgate_narrow,
        DK_B,
    )
    mixed = lax.psum_scatter(
        (
            jnp.dot(gated_w, readout_wide, preferred_element_type=jnp.float32)
            + jnp.dot(gated_n, readout_narrow, preferred_element_type=jnp.float32)
        ).astype(jnp.bfloat16),
        "tp",
        scatter_dimension=0,
        tiled=True,
    ).astype(jnp.float32)
    middle_f = (residual.astype(jnp.float32) + mixed).astype(jnp.bfloat16).astype(jnp.float32)
    normed = norm_rows(middle_f, norm_gain)
    all_rows = lax.all_gather(normed, "tp", axis=0, tiled=True)
    gate = jnp.dot(
        all_rows,
        lax.all_gather(gate_weight, "sp", axis=0, tiled=True),
        preferred_element_type=jnp.float32,
    )
    upper = jnp.dot(
        all_rows,
        lax.all_gather(up_weight, "sp", axis=0, tiled=True),
        preferred_element_type=jnp.float32,
    )
    hidden = (jax.nn.silu(gate) * upper).astype(jnp.bfloat16)
    terms = jnp.dot(
        hidden,
        lax.all_gather(down_weight, "sp", axis=1, tiled=True),
        preferred_element_type=jnp.float32,
    )
    back = lax.psum_scatter(
        terms.astype(jnp.bfloat16), "tp", scatter_dimension=0, tiled=True
    ).astype(jnp.float32)
    return (middle_f + back).astype(jnp.bfloat16)


def solution(mesh):
    in_specs = (
        P(("sp", "tp"), None),
        P("sp", "tp"),
        P("sp", "tp"),
        P("sp", "tp"),
        P("sp", "tp"),
        P(None, "tp", "sp"),
        P("tp"),
        P("tp", None),
        P("sp", "tp"),
        P("sp", "tp"),
        P("sp", "tp"),
        P("sp", "tp"),
        P(None, "tp", "sp"),
        P("tp"),
        P("tp", None),
        P(),
        P("sp", "tp"),
        P("sp", "tp"),
        P("tp", "sp"),
    )
    out_specs = P(("sp", "tp"), None)
    return jax.shard_map(body, mesh=mesh, in_specs=in_specs, out_specs=out_specs, check_vma=False)
```

profile of v0, /device:TPU:0, one launch (start us, length us, event | category | flops | bytes accessed | tf_op | source)
XLA Modules:
  0.0 764.9 jit_solution(13011065428079746588)
XLA Ops:
  10.6 5.3 while.55
  19.7 19.3 %while.54 = (s32[]{:T(128)}, f32[4,128,256]{2,1,0:T(8,128)S(1)}, f32[4]{0:T(128)}, f32[2,64,4,256]{3,1,0,2:T(8,128)}, f32[2,4,64]{2,1,0:T(4,128)}, /*index=5*/f3...) while((s32[]{:T(128)}, f32[4,128,256]{2,1,0:T(8,128)S(1)}, ...), condition=%wide.region_4.5_spmd.clone, body=%wide.region_0.4_spmd.clone.sunk | while | flops 130980880 | bytes 3455009 | solution.py:75
  21.8 1.3 add_maximum_fusion.4
  27.8 1.3 fusion.153
  31.8 1.3 add_maximum_fusion.4
  40.0 1.6 copy.70
  48.0 44.1 %all-reduce.4 = (f32[64]{0:T(128)S(1)}, f32[64]{0:T(128)S(1)}, f32[64]{0:T(128)S(1)}, f32[64]{0:T(128)S(1)}) all-reduce(f32[64]{0:T(128)S(1)} %dynamic-update-slice, f32[64]{0:T(128)S(1)} %dynamic-update-slice.1, f32[64]{0:T(128)S(1)} %dynamic-update-slice.2, f32[64]{0:T(128)S(1)} %dynamic-update-slice.3), channel_id=2, replica_groups=mesh['sp'=16,'tp'=2] {'sp'}, use_global_device_ids=true, to_apply=%add | all-reduce | flops 256 | bytes 2048
  101.2 93.0 %all-gather.18.cloned.1.call-done = f32[64,128,256]{2,1,0:T(8,128)} async-done(((f32[4,128,256]{2,1,0:T(8,128)}), f32[64,128,256]{2,1,0:T(8,128)}) %all-gather.18.cloned.1.call-update) | async-done | bytes 8388624 | tf_op jit(solution)/shard_map/all_gather | solution.py:13
  194.2 56.7 %while.56 = (s32[]{:T(128)}, f32[4,128,256]{2,1,0:T(8,128)S(1)}, f32[4]{0:T(128)}, f32[4,64,128]{2,1,0:T(8,128)S(1)}, f32[4]{0:T(128)}, /*index=5*/s32[]{:T(128)...) while((s32[]{:T(128)}, f32[4,128,256]{2,1,0:T(8,128)S(1)}, ...), condition=%wide.region_13.14_spmd.clone, body=%wide.region_12.13_spmd.clone.sunk | while | flops 819260 | bytes 1966609 | solution.py:25
  197.8 1.3 broadcast_select_fusion.9
  201.3 1.3 broadcast_select_fusion.9
  204.9 1.3 broadcast_select_fusion.9
  208.4 1.3 broadcast_select_fusion.9
  212.0 1.3 broadcast_select_fusion.9
  215.5 1.3 broadcast_select_fusion.9
  219.1 1.3 broadcast_select_fusion.9
  226.2 1.3 broadcast_select_fusion.9
  229.7 1.3 broadcast_select_fusion.9
  233.2 1.3 broadcast_select_fusion.9
  247.4 1.3 broadcast_select_fusion.9
  254.8 1.5 multiply_reduce_fusion
  256.7 3.0 fusion.76
  259.8 1.3 fusion.67
  262.9 4.4 reduce-scatter.3.cloned.1.call-done
  269.6 2.4 all_gather.52
  272.0 140.6 %all-gather.12.cloned.1.call-done = bf16[2048,2816]{1,0:T(8,128)(2,1)} async-done(((bf16[128,2816]{1,0:T(8,128)(2,1)}), bf16[2048,2816]{1,0:T(8,128)(2,1)}) %all-gather.12.cloned.1.call-update) | async-done | bytes 11534352 | tf_op jit(solution)/shard_map/all_gather | solution.py:185
  412.5 7.1 fusion.118
  419.6 135.2 %all-gather.14.cloned.1.call-done = bf16[2048,2816]{1,0:T(8,128)(2,1)} async-done(((bf16[128,2816]{1,0:T(8,128)(2,1)}), bf16[2048,2816]{1,0:T(8,128)(2,1)}) %all-gather.14.cloned.1.call-update) | async-done | bytes 11534352 | tf_op jit(solution)/shard_map/all_gather | solution.py:190
  554.8 182.8 %all-gather.16.cloned.1.call-done = bf16[2816,2048]{1,0:T(8,128)(2,1)} async-done(((bf16[2816,128]{1,0:T(8,128)(2,1)}), bf16[2816,2048]{1,0:T(8,128)(2,1)}) %all-gather.16.cloned.1.call-update) | async-done | bytes 11534352 | tf_op jit(solution)/shard_map/all_gather | solution.py:196
  737.6 12.4 %convolution_convert_fusion = bf16[128,2048]{1,0:T(8,128)(2,1)} fusion(bf16[2816,2048]{1,0:T(8,128)(2,1)} %all-gather.16.cloned.1.call-done, bf16[128,2048]{1,0:T(8,128)(2,1)S(1)} %all_gather.52, bf16[2048,2816]{1,0:T(8,128)(2,1)} %all-gather.14.cloned.1.call-done, f32[128,2816]{1,0:T(8,128)} %fusion.118), kind=kOutput, calls=%fused_computation.130 | convolution fusion | flops 2955214848 | bytes 25559040 | tf_op jit(solution)/shard_map/dot_general | solution.py:194
  750.0 6.3 reduce-scatter.5.cloned.1.call-done
  756.3 1.7 fusion.75
  (256 shorter events, 94.1 us)
Async XLA Ops:
  6.5 253.2 %copy-start = (bf16[512,2048]{1,0:T(8,128)(2,1)S(1)}, bf16[512,2048]{1,0:T(8,128)(2,1)}, u32[]{:S(2)}) copy-start(bf16[512,2048]{1,0:T(8,128)(2,1)} %param.39) | copy-start | bytes 6291460
  6.5 94.7 %all-gather.20.cloned.1.call-start = ((), (), s32[]{:S(2)}) async-start(), calls=%async_computation.8 | async-start | bytes 2228224 | tf_op jit(solution)/shard_map/all_gather | solution.py:13
  10.6 6.1 copy-start.15
  10.6 7.0 copy-start.8
  10.6 7.1 copy-start.11
  10.6 7.2 copy-start.7
  15.9 0.6 copy-start.3
  15.9 1.6 copy-start.12
  15.9 1.6 copy-start.16
  16.6 177.6 %all-gather.18.cloned.1.call-start = ((), (), s32[]{:S(2)}) async-start(), calls=%async_computation.7 | async-start | bytes 8912896 | tf_op jit(solution)/shard_map/all_gather | solution.py:13
  20.4 2.7 copy-start.6
  21.0 2.1 copy-start.9
  29.8 3.3 copy-start.6
  31.0 2.1 copy-start.9
  39.0 0.8 copy-start.2
  39.9 227.5 %reduce-scatter.3.cloned.1.call-start = ((), (), s32[]{:S(2)}) async-start(), calls=%async_computation.2 | async-start | bytes 786432 | tf_op jit(solution)/shard_map/reduce_scatter | solution.py:171
  46.1 51.3 %copy-start.13 = (f32[4,128]{1,0:T(4,128)}, f32[4,128]{1,0:T(4,128)S(1)}, u32[]{:S(2)}) copy-start(f32[4,128]{1,0:T(4,128)S(1)} %reduce_window_sum.38) | copy-start | bytes 6148
  47.5 49.9 %copy-start.14 = (f32[4,128]{1,0:T(4,128)}, f32[4,128]{1,0:T(4,128)S(1)}, u32[]{:S(2)}) copy-start(f32[4,128]{1,0:T(4,128)S(1)} %reduce_window_sum.39) | copy-start | bytes 6148
  251.0 5.7 copy-start.19
  256.4 3.3 copy-start.10
  256.4 3.3 copy-start.17
  259.7 3.2 copy-start.18
  259.7 7.6 copy-start.4
  261.1 151.4 %all-gather.12.cloned.1.call-start = ((), (), s32[]{:S(2)}) async-start(), calls=%async_computation.3 | async-start | bytes 12255232 | tf_op jit(solution)/shard_map/all_gather | solution.py:185
  261.7 293.1 %all-gather.14.cloned.1.call-start = ((), (), s32[]{:S(2)}) async-start(), calls=%async_computation.4 | async-start | bytes 12255232 | tf_op jit(solution)/shard_map/all_gather | solution.py:190
  262.3 475.3 %all-gather.16.cloned.1.call-start = ((), (), s32[]{:S(2)}) async-start(), calls=%async_computation.5 | async-start | bytes 12255232 | tf_op jit(solution)/shard_map/all_gather | solution.py:196
  262.8 493.5 %reduce-scatter.5.cloned.1.call-start = ((), (), s32[]{:S(2)}) async-start(), calls=%async_computation.6 | async-start | bytes 786432 | tf_op jit(solution)/shard_map/reduce_scatter | solution.py:199
  419.6 336.7 %copy-start.5 = (bf16[64,2048]{1,0:T(8,128)(2,1)S(1)}, bf16[64,2048]{1,0:T(8,128)(2,1)}, u32[]{:S(2)}) copy-start(bf16[64,2048]{1,0:T(8,128)(2,1)} %reduce-scatter.3.cloned.1.call-done) | copy-start | bytes 786436
  737.6 20.5 %copy-start.1 = (bf16[512,2048]{1,0:T(8,128)(2,1)S(1)}, bf16[512,2048]{1,0:T(8,128)(2,1)}, u32[]{:S(2)}) copy-start(bf16[512,2048]{1,0:T(8,128)(2,1)} %param.39) | copy-start | bytes 6291460
Sparse Core Ops, SparseCore 0:
  16.7 63.6 all-gather.19
  83.2 111.0 all-gather.17
  261.2 6.0 reduce-scatter.2
  270.0 142.5 all-gather.11
  415.1 139.5 all-gather.13
  557.3 180.2 all-gather.15
  750.2 6.0 reduce-scatter.4
where the time goes:
time: 768 us; the launch traced here: 765 us
  waiting for transfers between devices  564 us (73%)
  other arithmetic  79.1 us (10%)
  blocking collectives  46.5 us (6%)
  matrix products  35.6 us (5%)
  local copies, waits for them, and re-layouts  24.3 us (3%)
  between operations  14.5 us (2%)
    all_gather x1, waiting for transfers between devices, body(): lax.all_gather(down_weight, 'sp', axis=1, tiled=True)  183 us
    all_gather x1, waiting for transfers between devices, body(): lax.all_gather(gate_weight, 'sp', axis=0, tiled=True)  141 us
    all_gather x1, waiting for transfers between devices, body(): lax.all_gather(up_weight, 'sp', axis=0, tiled=True)  135 us
    all_gather x2, waiting for transfers between devices, entering(): everything = jax.tree.map(lambda part: lax.all_gather(part, axis), value)  93 us
    select_n x48, other arithmetic, step(): return jax.tree.map(lambda a, b: jnp.where(reached, a, b), new, before)  55.7 us
    unnamed x1, blocking collectives  44.1 us
  transfers between devices with their start and end apart: 7, of which 6 were waited for; matrix products, arithmetic and copies ran while one was open for 6% of the time, Pallas kernels for 0%

commit v1 on v0

--- a/solution.py
+++ b/solution.py
@@ -6,6 +6,13 @@
 DK_A = 128
 DK_B = 64
 BLOCK = 64
+
+
+def gather_over(x, axis, d):
+    size = lax.axis_size(axis)
+    blocks = jnp.stack([x for _ in range(size)])
+    blocks = lax.all_to_all(blocks, axis, split_axis=0, concat_axis=0)
+    return jnp.concatenate(blocks, axis=d)
 
 
 def entering(value, axis, combine, identity):
@@ -180,11 +187,7 @@
     middle_f = (residual.astype(jnp.float32) + mixed).astype(jnp.bfloat16).astype(jnp.float32)
     normed = norm_rows(middle_f, norm_gain)
     all_rows = lax.all_gather(normed, "tp", axis=0, tiled=True)
-    gate = jnp.dot(
-        all_rows,
-        lax.all_gather(gate_weight, "sp", axis=0, tiled=True),
-        preferred_element_type=jnp.float32,
-    )
+    gate = jnp.dot(all_rows, gather_over(gate_weight, "sp", 0), preferred_element_type=jnp.float32)
     upper = jnp.dot(
         all_rows,
         lax.all_gather(up_weight, "sp", axis=0, tiled=True),

time: 768 us -> 836 us (1.089)
  waiting for transfers between devices: 564 us -> 622 us
    all_to_all x0 -> x1, waiting for transfers between devices: none -> 260 us  [gather_over(): blocks = lax.all_to_all(blocks, axis, split_axis=0, concat_axis=0)]
    all_gather x1 -> x0, waiting for transfers between devices: 141 us -> none  [body(): lax.all_gather(gate_weight, 'sp', axis=0, tiled=True)]
    all_gather x1, waiting for transfers between devices: 135 us -> 71.1 us  [body(): lax.all_gather(up_weight, 'sp', axis=0, tiled=True)]
  transfers between devices with their start and end apart: 7 -> 7, of which waited for: 6 -> 5; matrix products, arithmetic and copies ran while one was open for 6% -> 6% of each run, Pallas kernels for 0% -> 0%
where the time goes in v1:
time: 836 us; the launch traced here: 833 us
  waiting for transfers between devices  622 us (74%)
  other arithmetic  79.1 us (9%)
  blocking collectives  46.5 us (6%)
  matrix products  35.6 us (4%)
  local copies, waits for them, and re-layouts  29.6 us (4%)
  between operations  14.6 us (2%)
    all_to_all x1, waiting for transfers between devices, gather_over(): blocks = lax.all_to_all(blocks, axis, split_axis=0, concat_axis=0)  260 us
    all_gather x1, waiting for transfers between devices, body(): lax.all_gather(down_weight, 'sp', axis=1, tiled=True)  191 us
    all_gather x2, waiting for transfers between devices, entering(): everything = jax.tree.map(lambda part: lax.all_gather(part, axis), value)  93 us
    all_gather x1, waiting for transfers between devices, body(): lax.all_gather(up_weight, 'sp', axis=0, tiled=True)  71.1 us
    select_n x48, other arithmetic, step(): return jax.tree.map(lambda a, b: jnp.where(reached, a, b), new, before)  55.7 us
    unnamed x1, blocking collectives  44.1 us
  transfers between devices with their start and end apart: 7, of which 5 were waited for; matrix products, arithmetic and copies ran while one was open for 6% of the time, Pallas kernels for 0%

profile of v1, /device:TPU:0, one launch (start us, length us, event | category | flops | bytes accessed | tf_op | source)
XLA Modules:
  0.0 833.5 jit_solution(12622609114890847662)
XLA Ops:
  10.6 5.3 while.55
  19.7 19.3 %while.54 = (s32[]{:T(128)}, f32[4,128,256]{2,1,0:T(8,128)S(1)}, f32[4]{0:T(128)}, f32[2,64,4,256]{3,1,0,2:T(8,128)}, f32[2,4,64]{2,1,0:T(4,128)}, /*index=5*/f3...) while((s32[]{:T(128)}, f32[4,128,256]{2,1,0:T(8,128)S(1)}, ...), condition=%wide.region_4.5_spmd.clone, body=%wide.region_0.4_spmd.clone.sunk | while | flops 130980880 | bytes 3455009 | solution.py:82
  21.8 1.3 add_maximum_fusion.4
  27.8 1.3 fusion.153
  31.8 1.3 add_maximum_fusion.4
  40.0 1.6 copy.70
  48.0 44.1 %all-reduce.4 = (f32[64]{0:T(128)S(1)}, f32[64]{0:T(128)S(1)}, f32[64]{0:T(128)S(1)}, f32[64]{0:T(128)S(1)}) all-reduce(f32[64]{0:T(128)S(1)} %dynamic-update-slice, f32[64]{0:T(128)S(1)} %dynamic-update-slice.1, f32[64]{0:T(128)S(1)} %dynamic-update-slice.2, f32[64]{0:T(128)S(1)} %dynamic-update-slice.3), channel_id=2, replica_groups=mesh['sp'=16,'tp'=2] {'sp'}, use_global_device_ids=true, to_apply=%add | all-reduce | flops 256 | bytes 2048
  101.2 93.0 %all-gather.15.cloned.1.call-done = f32[64,128,256]{2,1,0:T(8,128)} async-done(((f32[4,128,256]{2,1,0:T(8,128)}), f32[64,128,256]{2,1,0:T(8,128)}) %all-gather.15.cloned.1.call-update) | async-done | bytes 8388624 | tf_op jit(solution)/shard_map/all_gather | solution.py:20
  194.2 56.7 %while.56 = (s32[]{:T(128)}, f32[4,128,256]{2,1,0:T(8,128)S(1)}, f32[4]{0:T(128)}, f32[4,64,128]{2,1,0:T(8,128)S(1)}, f32[4]{0:T(128)}, /*index=5*/s32[]{:T(128)...) while((s32[]{:T(128)}, f32[4,128,256]{2,1,0:T(8,128)S(1)}, ...), condition=%wide.region_13.14_spmd.clone, body=%wide.region_12.13_spmd.clone.sunk | while | flops 819260 | bytes 1966609 | solution.py:32
  197.8 1.3 broadcast_select_fusion.9
  201.3 1.3 broadcast_select_fusion.9
  204.9 1.3 broadcast_select_fusion.9
  208.4 1.3 broadcast_select_fusion.9
  212.0 1.3 broadcast_select_fusion.9
  215.5 1.3 broadcast_select_fusion.9
  219.1 1.3 broadcast_select_fusion.9
  226.2 1.3 broadcast_select_fusion.9
  229.7 1.3 broadcast_select_fusion.9
  233.2 1.3 broadcast_select_fusion.9
  254.8 1.5 multiply_reduce_fusion
  256.7 3.0 fusion.76
  259.7 1.3 fusion.67
  261.7 5.3 stack.2
  266.9 5.0 all-to-all-start
  274.9 2.4 all_gather.49
  277.2 259.9 %all-to-all-done = bf16[16,128,2816]{2,1,0:T(8,128)(2,1)} async-done(((bf16[16,128,2816]{2,1,0:T(8,128)(2,1)}), bf16[16,128,2816]{2,1,0:T(8,128)(2,1)}, u32[]{:S(2)}, u32[]{:S(2)}) %all-to-all-start) | async-done | bytes 11534368 | tf_op jit(solution)/shard_map/all_to_all | solution.py:14
  537.2 7.1 fusion.118
  544.2 71.1 %all-gather.11.cloned.1.call-done = bf16[2048,2816]{1,0:T(8,128)(2,1)} async-done(((bf16[128,2816]{1,0:T(8,128)(2,1)}), bf16[2048,2816]{1,0:T(8,128)(2,1)}) %all-gather.11.cloned.1.call-update) | async-done | bytes 11534352 | tf_op jit(solution)/shard_map/all_gather | solution.py:193
  615.4 190.7 %all-gather.13.cloned.1.call-done = bf16[2816,2048]{1,0:T(8,128)(2,1)} async-done(((bf16[2816,128]{1,0:T(8,128)(2,1)}), bf16[2816,2048]{1,0:T(8,128)(2,1)}) %all-gather.13.cloned.1.call-update) | async-done | bytes 11534352 | tf_op jit(solution)/shard_map/all_gather | solution.py:199
  806.1 12.4 %convolution_convert_fusion = bf16[128,2048]{1,0:T(8,128)(2,1)} fusion(bf16[2816,2048]{1,0:T(8,128)(2,1)} %all-gather.13.cloned.1.call-done, bf16[128,2048]{1,0:T(8,128)(2,1)S(1)} %all_gather.49, bf16[2048,2816]{1,0:T(8,128)(2,1)} %all-gather.11.cloned.1.call-done, f32[128,2816]{1,0:T(8,128)} %fusion.118), kind=kOutput, calls=%fused_computation.130 | convolution fusion | flops 2955214848 | bytes 25559040 | tf_op jit(solution)/shard_map/dot_general | solution.py:197
  818.6 6.3 reduce-scatter.5.cloned.1.call-done
  824.9 1.7 fusion.75
  (258 shorter events, 94.8 us)
Async XLA Ops:
  6.5 253.2 %copy-start = (bf16[512,2048]{1,0:T(8,128)(2,1)S(1)}, bf16[512,2048]{1,0:T(8,128)(2,1)}, u32[]{:S(2)}) copy-start(bf16[512,2048]{1,0:T(8,128)(2,1)} %param.39) | copy-start | bytes 6291460
  6.5 94.7 %all-gather.17.cloned.1.call-start = ((), (), s32[]{:S(2)}) async-start(), calls=%async_computation.8 | async-start | bytes 2228224 | tf_op jit(solution)/shard_map/all_gather | solution.py:20
  10.6 6.1 copy-start.16
  10.6 7.0 copy-start.9
  10.6 7.1 copy-start.12
  10.6 7.2 copy-start.8
  15.9 0.6 copy-start.3
  15.9 1.6 copy-start.13
  15.9 1.6 copy-start.17
  16.6 177.6 %all-gather.15.cloned.1.call-start = ((), (), s32[]{:S(2)}) async-start(), calls=%async_computation.7 | async-start | bytes 8912896 | tf_op jit(solution)/shard_map/all_gather | solution.py:20
  20.4 2.7 copy-start.6
  21.0 2.1 copy-start.10
  29.8 3.3 copy-start.6
  31.0 2.1 copy-start.10
  39.0 0.8 copy-start.2
  39.9 232.8 %reduce-scatter.3.cloned.1.call-start = ((), (), s32[]{:S(2)}) async-start(), calls=%async_computation.3 | async-start | bytes 786432 | tf_op jit(solution)/shard_map/reduce_scatter | solution.py:178
  46.1 51.3 %copy-start.14 = (f32[4,128]{1,0:T(4,128)}, f32[4,128]{1,0:T(4,128)S(1)}, u32[]{:S(2)}) copy-start(f32[4,128]{1,0:T(4,128)S(1)} %reduce_window_sum.38) | copy-start | bytes 6148
  47.5 49.9 %copy-start.15 = (f32[4,128]{1,0:T(4,128)}, f32[4,128]{1,0:T(4,128)S(1)}, u32[]{:S(2)}) copy-start(f32[4,128]{1,0:T(4,128)S(1)} %reduce_window_sum.39) | copy-start | bytes 6148
  251.0 5.7 copy-start.20
  256.4 3.3 copy-start.11
  256.4 3.3 copy-start.18
  259.7 1.9 copy-start.7
  261.1 354.3 %all-gather.11.cloned.1.call-start = ((), (), s32[]{:S(2)}) async-start(), calls=%async_computation.4 | async-start | bytes 12255232 | tf_op jit(solution)/shard_map/all_gather | solution.py:193
  266.9 5.7 copy-start.19
  266.9 5.7 copy-start.4
  266.9 270.2 %all-to-all-start = ((bf16[16,128,2816]{2,1,0:T(8,128)(2,1)}), bf16[16,128,2816]{2,1,0:T(8,128)(2,1)}, u32[]{:S(2)}, u32[]{:S(2)}) async-start(bf16[16,128,2816]{2,1,0:T(8,128)(2,1)} %stack.2), calls=%async_computation.1 | async-start | bytes 23068672 | tf_op jit(solution)/shard_map/all_to_all | solution.py:14
  272.0 534.2 %all-gather.13.cloned.1.call-start = ((), (), s32[]{:S(2)}) async-start(), calls=%async_computation.5 | async-start | bytes 12255232 | tf_op jit(solution)/shard_map/all_gather | solution.py:199
  272.5 552.3 %reduce-scatter.5.cloned.1.call-start = ((), (), s32[]{:S(2)}) async-start(), calls=%async_computation.6 | async-start | bytes 786432 | tf_op jit(solution)/shard_map/reduce_scatter | solution.py:202
  544.2 280.6 %copy-start.5 = (bf16[64,2048]{1,0:T(8,128)(2,1)S(1)}, bf16[64,2048]{1,0:T(8,128)(2,1)}, u32[]{:S(2)}) copy-start(bf16[64,2048]{1,0:T(8,128)(2,1)} %reduce-scatter.3.cloned.1.call-done) | copy-start | bytes 786436
  806.1 20.5 %copy-start.1 = (bf16[512,2048]{1,0:T(8,128)(2,1)S(1)}, bf16[512,2048]{1,0:T(8,128)(2,1)}, u32[]{:S(2)}) copy-start(bf16[512,2048]{1,0:T(8,128)(2,1)} %param.39) | copy-start | bytes 6291460
Sparse Core Ops, SparseCore 0:
  16.7 63.6 all-gather.16
  83.2 111.0 all-gather.14
  261.2 6.0 reduce-scatter.2
  269.9 345.3 all-gather.10
  617.9 188.1 all-gather.12
  818.7 6.0 reduce-scatter.4
